TPU v7x, 32 devices: a whole 2x2x4 slice. The times are simulated.
32 devices in a mesh: ep: 8 (over z, x), tp: 4 (over y, core).
Axes of the slice: x: 2, y: 2, z: 4, core: 2. Of those that a mesh axis runs over, the one named last changes fastest.
Arguments:
- queries: bfloat16 [2048, 8, 128], P('ep', 'tp'), may hold values from -256 to 256
- keys: bfloat16 [2048, 4, 128], P('ep', 'tp'), may hold values from -8 to 8
- values: bfloat16 [2048, 4, 128], P('ep', 'tp'), may hold values from -6 to 6
- attn_lambda: float32 [8], P('tp'), may hold values from 0.3 to 0.8
- head_gain: float32 [128], replicated, may hold values from 0.1 to 1.9
- w_out: bfloat16 [1024, 2048], replicated, may hold values from -0.1875 to 0.1875
- moe_rows: bfloat16 [4096, 2048], P('ep'), may hold values from -6 to 6
- moe_gain: float32 [2048], replicated, may hold values from 0.1 to 1.9
- routes: int32 [4096, 2], P('ep'), may hold values from 0 to 7, all different within a row; in each aligned block of 128 rows (0 to 127, 128 to 255, ...) at most 64 rows name the same one
- route_weights: float32 [4096, 2], P('ep'), may hold values from 0.1 to 1
- w_gate: bfloat16 [8, 2048, 1024], P('ep', None, 'tp'), may hold values from -0.125 to 0.125
- w_up: bfloat16 [8, 2048, 1024], P('ep', None, 'tp'), may hold values from -0.125 to 0.125
- w_down: bfloat16 [8, 1024, 2048], P('ep', 'tp'), may hold values from -0.1875 to 0.1875
Outputs:
- mixer_out: bfloat16 [2048, 2048], P(('ep', 'tp'))
- moe_out: bfloat16 [4096, 2048], P(('ep', 'tp'))
Inputs may be any that keep to these rules, and one draw needn't show every extreme that they name: `routes`: each row names 2 different experts. In each aligned block of 128 rows (the rows of moe_out that one device holds) no expert is named by more than 64 rows, a bound that some block reaches.
All inputs are finite; a program needn't handle non-finite values.
Results may differ from a plain program's by a relative error of at most 0.011.
Values may be sent and summed in bfloat16 or wider, within the bound.
A program may use at most 128 MiB of HBM per device.

v0:
```python
import jax
import jax.numpy as jnp
from jax import lax
from jax.sharding import PartitionSpec as P

EPSILON = 1e-06
MASKED = -1e30


def rms_scaled(values_f, gain):
    mean_sq = jnp.mean(values_f * values_f, axis=-1, keepdims=True)
    return values_f * lax.rsqrt(mean_sq + EPSILON) * gain


def slot_numbers(block_routes, experts):
    flat_ids = block_routes.reshape(-1)
    matches = (flat_ids[:, None] == lax.iota(jnp.int32, experts)[None, :]).astype(jnp.int32)
    earlier = jnp.cumsum(matches, axis=0) - matches
    return jnp.sum(earlier * matches, axis=1).reshape(block_routes.shape)


def fill_slots(block_rows, block_routes, experts, capacity):
    slot_ids = slot_numbers(block_routes, experts)
    model_width = block_rows.shape[1]
    copies = jnp.broadcast_to(block_rows[:, None, :], block_routes.shape + (model_width,))
    blank_slots = jnp.zeros((experts, capacity, model_width), block_rows.dtype)
    return (blank_slots.at[block_routes, slot_ids].set(copies), slot_ids)


def local(
    queries,
    keys,
    values,
    attn_lambda,
    head_gain,
    w_out,
    moe_rows,
    moe_gain,
    routes,
    route_weights,
    w_gate,
    w_up,
    w_down,
):
    positions = queries.shape[0]
    q_heads = queries.shape[1]
    kv_heads = keys.shape[1]
    head_dim = queries.shape[2] // 2
    value_dim = values.shape[2]
    per_key = q_heads // kv_heads
    first_pos = lax.axis_index("ep") * positions
    query_pos = first_pos + lax.iota(jnp.int32, positions)
    last_pos = first_pos + positions - 1
    query_view = queries.reshape(positions, kv_heads, per_key, 2, head_dim)
    inv_scale = head_dim ** (-0.5)
    start_max = jnp.full((positions, kv_heads, per_key, 2), MASKED, jnp.float32)
    start_total = jnp.zeros((positions, kv_heads, per_key, 2), jnp.float32)
    start_acc = jnp.zeros((positions, kv_heads, per_key, 2, value_dim), jnp.float32)
    carry = (start_max, start_total, start_acc)
    key_piece = lax.all_gather(keys, "ep", axis=0, tiled=True)
    value_piece = lax.all_gather(values, "ep", axis=0, tiled=True)
    shard_count = key_piece.shape[0] // positions
    together = 1
    for candidate in (2, 3, 4):
        if shard_count % candidate == 0:
            together = candidate
    block_len = together * positions
    blocks = shard_count // together
    key_blocks = key_piece.reshape(blocks, block_len, kv_heads, 2, head_dim)
    value_blocks = value_piece.reshape(blocks, block_len, kv_heads, value_dim)
    block_starts = block_len * lax.iota(jnp.int32, blocks)

    def visit(running, inputs):
        key_blk, value_blk, block_start = inputs

        def update(current):
            run_max, run_total, run_acc = current
            key_pos = block_start + lax.iota(jnp.int32, block_len)
            scores = (
                jnp.einsum(
                    "qkgmd,pkmd->qkgmp", query_view, key_blk, preferred_element_type=jnp.float32
                )
                * inv_scale
            )
            allowed = key_pos[None, :] <= query_pos[:, None]
            scores = jnp.where(allowed[:, None, None, None, :], scores, MASKED)
            new_max = jnp.maximum(run_max, jnp.max(scores, axis=-1))
            shrink = jnp.exp(run_max - new_max)
            weights = jnp.exp(scores - new_max[..., None])
            run_total = run_total * shrink + jnp.sum(weights, axis=-1)
            run_acc = run_acc * shrink[..., None] + jnp.einsum(
                "qkgmp,pkv->qkgmv",
                weights.astype(jnp.bfloat16),
                value_blk,
                preferred_element_type=jnp.float32,
            )
            return (new_max, run_total, run_acc)

        def keep(current):
            return current

        return (lax.cond(block_start <= last_pos, update, keep, running), None)

    carry, unused = lax.scan(visit, carry, (key_blocks, value_blocks, block_starts))
    run_max, run_total, run_acc = carry
    ratios = run_acc / run_total[..., None]
    lambda_view = attn_lambda.reshape(1, kv_heads, per_key, 1)
    head_out = ratios[:, :, :, 0] - lambda_view * ratios[:, :, :, 1]
    attn_rows = (
        rms_scaled(head_out, head_gain).astype(jnp.bfloat16).reshape(positions, q_heads * value_dim)
    )
    tp_count = lax.axis_size("tp")
    tp_id = lax.axis_index("tp")
    exchanged = lax.all_to_all(
        attn_rows.reshape(positions, q_heads, value_dim),
        "tp",
        split_axis=0,
        concat_axis=1,
        tiled=True,
    )
    mixer_out = jnp.dot(
        exchanged.reshape(positions // tp_count, tp_count * q_heads * value_dim),
        w_out,
        preferred_element_type=jnp.float32,
    ).astype(jnp.bfloat16)
    experts = lax.axis_size("ep")
    dev_rows = moe_rows.shape[0] // tp_count
    top_count = routes.shape[1]
    capacity = max(2, 2 * dev_rows * top_count // experts)
    model_width = moe_rows.shape[1]
    hidden_units = w_gate.shape[2]
    own_routes = lax.dynamic_slice_in_dim(routes, tp_id * dev_rows, dev_rows, 0)
    own_weights = lax.dynamic_slice_in_dim(route_weights, tp_id * dev_rows, dev_rows, 0)
    own_rows = rms_scaled(
        lax.dynamic_slice_in_dim(moe_rows, tp_id * dev_rows, dev_rows, 0).astype(jnp.float32),
        moe_gain,
    ).astype(jnp.bfloat16)
    outgoing, own_slots = fill_slots(own_rows, own_routes, experts, capacity)
    arrived = lax.all_to_all(outgoing, "ep", split_axis=0, concat_axis=0, tiled=True)
    slot_rows = lax.all_gather(arrived[None], "tp", axis=0, tiled=True)
    flat_rows = slot_rows.reshape(-1, model_width)
    gate_out = jnp.dot(flat_rows, w_gate[0], preferred_element_type=jnp.float32)
    up_out = jnp.dot(flat_rows, w_up[0], preferred_element_type=jnp.float32)
    hidden = (
        (jax.nn.silu(gate_out) * up_out)
        .astype(jnp.bfloat16)
        .reshape(slot_rows.shape[:-1] + (hidden_units,))
    )
    flat_terms = hidden.reshape(-1, hidden_units)
    summed = lax.psum_scatter(
        jnp.dot(flat_terms, w_down[0], preferred_element_type=jnp.float32)
        .reshape(hidden.shape[:-1] + (model_width,))
        .astype(jnp.bfloat16),
        "tp",
        scatter_dimension=0,
        tiled=True,
    )
    returned = lax.all_to_all(summed, "ep", split_axis=1, concat_axis=1, tiled=True)[0]
    picked = returned[own_routes, own_slots]
    moe_out = jnp.sum(own_weights[..., None] * picked.astype(jnp.float32), axis=1).astype(
        jnp.bfloat16
    )
    return (mixer_out, moe_out)


def solution(mesh):
    return jax.shard_map(
        local,
        mesh=mesh,
        in_specs=(
            P("ep", "tp", None),
            P("ep", "tp", None),
            P("ep", "tp", None),
            P("tp"),
            P(),
            P(),
            P("ep", None),
            P(),
            P("ep", None),
            P("ep", None),
            P("ep", None, "tp"),
            P("ep", None, "tp"),
            P("ep", "tp", None),
        ),
        out_specs=(P(("ep", "tp"), None), P(("ep", "tp"), None)),
        check_vma=False,
    )
```

profile of v0, /device:TPU:0, one launch (start us, length us, event | category | flops | bytes accessed | tf_op | source)
XLA Modules:
  0.0 330.0 jit_solution(4695768976303798606)
XLA Ops:
  7.2 0.8 constant_dynamic-slice_fusion
  8.4 0.6 reduce-window.6
  9.7 1.2 fusion.24
  10.9 1.3 fusion.26
  12.2 0.6 broadcast_in_dim.60
  12.8 1.2 reshape.233
  14.3 33.4 %scatter_fusion = bf16[8,64,2048]{2,1,0:T(8,128)(2,1)S(1)} fusion(bf16[8,64,2048]{2,1,0:T(8,128)(2,1)S(1)} %broadcast_in_dim.58, s32[256]{0:T(256)S(1)} %reshape.231, bf16[256,2048]{1,0:T(8,128)(2,1)} %reshape.233), kind=kCustom, calls=%fused_computation.1 | custom fusion | bytes 3147776 | tf_op jit(solution)/shard_map/scatter | solution.py:27
  47.7 55.4 %all_to_all.25 = bf16[8,64,2048]{2,1,0:T(8,128)(2,1)} all-to-all(bf16[8,64,2048]{2,1,0:T(8,128)(2,1)S(1)} %scatter_fusion), channel_id=1, replica_groups=mesh['ep'=8,'tp'=4] {'ep'}, dimensions={0} | all-to-all | bytes 4194304 | tf_op jit(solution)/shard_map/all_to_all | solution.py:139
  103.2 57.4 %all-gather.3.cloned.1.call-done = bf16[32,64,2048]{2,1,0:T(8,128)(2,1)} async-done(((bf16[8,64,2048]{2,1,0:T(8,128)(2,1)}), bf16[32,64,2048]{2,1,0:T(8,128)(2,1)}) %all-gather.3.cloned.1.call-update) | async-done | bytes 8388624 | tf_op jit(solution)/shard_map/all_gather | solution.py:140
  160.6 5.9 %fusion.29 = f32[2048,256]{1,0:T(8,128)S(1)} fusion(bf16[2048,2048]{1,0:T(8,128)(2,1)} %bitcast.134, bf16[1,2048,256]{2,1,0:T(8,128)(2,1)S(1)} %copy-done.7), kind=kOutput, calls=%fused_computation.40 | convolution fusion | flops 2147483648 | bytes 11534336 | tf_op jit(solution)/shard_map/dot_general | solution.py:142
  166.6 2.6 fusion.23
  169.2 5.6 %convolution_convert_fusion = bf16[4,8,64,2048]{3,2,1,0:T(8,128)(2,1)} fusion(bf16[4,8,64,256]{3,2,1,0:T(8,128)(2,1)S(1)} %bitcast.130, bf16[1,256,2048]{2,1,0:T(8,128)(2,1)S(1)} %copy-done), kind=kOutput, calls=%fused_computation.28 | convolution fusion | flops 2151677952 | bytes 10485760 | tf_op jit(solution)/shard_map/dot_general | solution.py:151
  174.8 0.8 copy-done.2
  175.6 31.4 %all_gather.9 = bf16[2048,1,128]{2,0,1:T(8,128)(2,1)S(1)} all-gather(bf16[256,1,128]{2,0,1:T(8,128)(2,1)S(1)} %copy-done.2), channel_id=1, replica_groups=mesh['ep'=8,'tp'=4] {'ep'}, dimensions={0}, use_global_device_ids=true | all-gather | bytes 589824 | tf_op jit(solution)/shard_map/all_gather | solution.py:60
  207.5 0.7 copy.64
  208.3 31.4 %all_gather.10 = bf16[2048,1,128]{2,0,1:T(8,128)(2,1)S(1)} all-gather(bf16[256,1,128]{2,0,1:T(8,128)(2,1)S(1)} %copy-done.3), channel_id=1, replica_groups=mesh['ep'=8,'tp'=4] {'ep'}, dimensions={0}, use_global_device_ids=true | all-gather | bytes 589824 | tf_op jit(solution)/shard_map/all_gather | solution.py:61
  240.1 5.6 %while.15 = (s32[]{:T(128)}, f32[256,1,2,2]{0,2,3,1:T(2,128)S(1)}, f32[256,1,2,2]{0,2,3,1:T(2,128)S(1)}, f32[256,1,2,2,128]{0,4,3,2,1:T(8,128)S(1)}, s32[2]{0:T(...) while((s32[]{:T(128)}, f32[256,1,2,2]{0,2,3,1:T(2,128)S(1)}, ...), condition=%wide.region_5.6_spmd.clone, body=%wide.region_0.5_spmd.clone.sunk | while | flops 411570432 | bytes 15155487 | solution.py:104
  240.2 0.6 dynamic_slice.50
  241.3 3.3 conditional.3
  241.3 0.6 iota_add_fusion
  242.1 0.9 fusion.4
  243.0 1.0 fusion.5
  244.6 0.6 dynamic_slice.50
  246.1 0.7 broadcast_divide_fusion
  247.8 7.0 %all_to_all.26 = bf16[256,2,128]{2,1,0:T(2,128)(2,1)S(1)} all-to-all(bf16[256,2,128]{2,1,0:T(2,128)(2,1)S(1)} %fusion.37), channel_id=1, replica_groups=mesh['ep'=8,'tp'=4] {'tp'}, dimensions={0} | all-to-all | bytes 262144 | tf_op jit(solution)/shard_map/all_to_all | solution.py:114
  254.8 8.9 %all-to-all-start.2 = ((bf16[1,8,64,2048]{3,2,0,1:T(8,128)(2,1)}), bf16[1,8,64,2048]{3,2,0,1:T(8,128)(2,1)S(1)}, u32[]{:S(2)}, u32[]{:S(2)}) async-start(bf16[1,8,64,2048]{3,2,0,1:T(8,128)(2,1)} %bitcast.127), calls=%async_computation.3 | async-start | bytes 4194304 | tf_op jit(solution)/shard_map/all_to_all | solution.py:158
  263.9 0.7 constant_dynamic-slice_fusion.1
  264.9 3.7 %convolution_convert_fusion.1 = bf16[64,2048]{1,0:T(8,128)(2,1)} fusion(bf16[64,1024]{1,0:T(8,128)(2,1)S(1)} %reshape.221, bf16[1024,2048]{1,0:T(8,128)(2,1)} %param.22), kind=kOutput, calls=%fused_computation.31 | convolution fusion | flops 268566528 | bytes 4587520 | tf_op jit(solution)/shard_map/dot_general | solution.py:121
  268.6 42.9 %all-to-all-done.2 = bf16[1,8,64,2048]{3,2,0,1:T(8,128)(2,1)S(1)} async-done(((bf16[1,8,64,2048]{3,2,0,1:T(8,128)(2,1)}), bf16[1,8,64,2048]{3,2,0,1:T(8,128)(2,1)S(1)}, u32[]{:S(2)}, u32[]{:S(2)}) %all-to-all-start.2) | async-done | bytes 2097184 | tf_op jit(solution)/shard_map/all_to_all | solution.py:158
  311.6 5.3 %gather_fusion = bf16[256,2048]{1,0:T(8,128)(2,1)} fusion(bf16[8,64,2048]{2,1,0:T(8,128)(2,1)S(1)} %bitcast.126, s32[256]{0:T(256)S(1)} %reshape.225), kind=kCustom, calls=%fused_computation | custom fusion | bytes 2099200 | tf_op jit(solution)/shard_map/gather | solution.py:159
  316.9 2.4 reshape.239
  319.3 3.9 %multiply_reduce_fusion = bf16[128,2048]{1,0:T(8,128)(2,1)} fusion(f32[128,2,2048]{2,1,0:T(2,128)S(1)} %reshape.239, f32[128,2]{1,0:T(8,128)S(1)} %copy.73), kind=kLoop, calls=%fused_computation.32 | loop fusion | flops 786432 | bytes 2622464 | tf_op jit(solution)/shard_map/reduce_sum | solution.py:160
  (63 shorter events, 4.9 us)
Async XLA Ops:
  7.2 162.1 %copy-start = (bf16[1,256,2048]{2,1,0:T(8,128)(2,1)S(1)}, bf16[1,256,2048]{2,1,0:T(8,128)(2,1)}, u32[]{:S(2)}) copy-start(bf16[1,256,2048]{2,1,0:T(8,128)(2,1)} %param.29) | copy-start | bytes 3145732
  7.2 153.4 %all-gather.3.cloned.1.call-start = ((), (), s32[]{:S(2)}) async-start(), calls=%async_computation.5 | async-start | bytes 10485760 | tf_op jit(solution)/shard_map/all_gather | solution.py:140
  103.1 57.5 %copy-start.7 = (bf16[1,2048,256]{2,1,0:T(8,128)(2,1)S(1)}, bf16[1,2048,256]{2,1,0:T(8,128)(2,1)}, u32[]{:S(2)}) copy-start(bf16[1,2048,256]{2,1,0:T(8,128)(2,1)} %param.27) | copy-start | bytes 3145732
  103.1 151.7 %reduce-scatter.2.cloned.1.call-start = ((), (), s32[]{:S(2)}) async-start(), calls=%async_computation.4 | async-start | bytes 10485760 | tf_op jit(solution)/shard_map/reduce_scatter | solution.py:150
  160.6 5.9 %copy-start.6 = (bf16[32,64,2048]{2,1,0:T(8,128)(2,1)S(1)}, bf16[32,64,2048]{2,1,0:T(8,128)(2,1)}, u32[]{:S(2)}) copy-start(bf16[32,64,2048]{2,1,0:T(8,128)(2,1)} %all-gather.3.cloned.1.call-done) | copy-start | bytes 25165828
  160.6 6.0 %copy-start.8 = (bf16[1,2048,256]{2,1,0:T(8,128)(2,1)S(1)}, bf16[1,2048,256]{2,1,0:T(8,128)(2,1)}, u32[]{:S(2)}) copy-start(bf16[1,2048,256]{2,1,0:T(8,128)(2,1)} %param.28) | copy-start | bytes 3145732
  174.8 0.8 copy-start.2
  174.8 33.4 %copy-start.3 = (bf16[256,1,128]{2,0,1:T(8,128)(2,1)S(1)}, bf16[256,1,128]{2,0,1:T(8,128)(2,1)}, u32[]{:S(2)}) copy-start(bf16[256,1,128]{2,0,1:T(8,128)(2,1)} %param.19) | copy-start | bytes 196612
  207.1 32.8 %copy-start.1 = (bf16[256,2,128]{2,1,0:T(2,128)(2,1)S(1)}, bf16[256,2,128]{2,1,0:T(2,128)(2,1)}, u32[]{:S(2)}) copy-start(bf16[256,2,128]{2,1,0:T(2,128)(2,1)} %param.17) | copy-start | bytes 393220
  245.7 1.1 copy-start.4
  245.7 1.6 copy-start.5
  254.8 56.8 %all-to-all-start.2 = ((bf16[1,8,64,2048]{3,2,0,1:T(8,128)(2,1)}), bf16[1,8,64,2048]{3,2,0,1:T(8,128)(2,1)S(1)}, u32[]{:S(2)}, u32[]{:S(2)}) async-start(bf16[1,8,64,2048]{3,2,0,1:T(8,128)(2,1)} %bitcast.127), calls=%async_computation.3 | async-start | bytes 4194304 | tf_op jit(solution)/shard_map/all_to_all | solution.py:158
Sparse Core Ops, SparseCore 0:
  103.2 57.2 all-gather.2
  174.9 71.3 reduce-scatter.1
where the time goes:
time: 331 us; the launch traced here: 330 us
  blocking collectives  125 us (38%)
  waiting for transfers between devices  100 us (30%)
  local copies, waits for them, and re-layouts  49.9 us (15%)
  matrix products  19.2 us (6%)
  between operations  14.4 us (4%)
  other arithmetic  10.6 us (3%)
  starting transfers between devices  9.02 us (3%)
    all_gather x1, waiting for transfers between devices, local(): slot_rows = lax.all_gather(arrived[None], 'tp', axis=0, tiled=True)  57.4 us
    all_to_all x1, blocking collectives, local(): lax.all_to_all(outgoing, 'ep', split_axis=0, concat_axis=0, tiled=True)  55.4 us
    all_to_all x1, waiting for transfers between devices, local(): lax.all_to_all(summed, 'ep', split_axis=1, concat_axis=1, tiled=True)[0]  42.9 us
    scatter x1, local copies, waits for them, and re-layouts, fill_slots(): return (blank_slots.at[block_routes, slot_ids].set(copies), slot_ids)  33.4 us
    all_gather x1, blocking collectives, local(): key_piece = lax.all_gather(keys, 'ep', axis=0, tiled=True)  31.4 us
    all_gather x1, blocking collectives, local(): value_piece = lax.all_gather(values, 'ep', axis=0, tiled=True)  31.4 us
    all_to_all x1, starting transfers between devices, local(): lax.all_to_all(summed, 'ep', split_axis=1, concat_axis=1, tiled=True)[0]  8.94 us
    all_to_all x1, blocking collectives, local(): lax.all_to_all(attn_rows.reshape(positions, q_heads, value_dim), 'tp', sp...  6.99 us
  transfers between devices with their start and end apart: 3, of which 2 were waited for; matrix products, arithmetic and copies ran while one was open for 4% of the time, Pallas kernels for 0%

commit v1 on v0

--- a/solution.py
+++ b/solution.py
@@ -57,8 +57,14 @@
     start_total = jnp.zeros((positions, kv_heads, per_key, 2), jnp.float32)
     start_acc = jnp.zeros((positions, kv_heads, per_key, 2, value_dim), jnp.float32)
     carry = (start_max, start_total, start_acc)
-    key_piece = lax.all_gather(keys, "ep", axis=0, tiled=True)
-    value_piece = lax.all_gather(values, "ep", axis=0, tiled=True)
+
+    def _post_spot(page, local_array):
+        r1 = jnp.concatenate([page, local_array], axis=1)
+        upper = jax.lax.all_gather(r1, "ep", axis=0, tiled=True)
+        back = jnp.split(upper, [page.shape[1]], axis=1)
+        return back
+
+    key_piece, value_piece = _post_spot(keys, values)
     shard_count = key_piece.shape[0] // positions
     together = 1
     for candidate in (2, 3, 4):

time: 331 us -> 349 us (1.054)
  waiting for transfers between devices: 100 us -> 182 us
  blocking collectives: 125 us -> 62.6 us
    all_gather x2 -> x0, blocking collectives: 62.9 us -> none  [the longest x1 31.4 us: local(): key_piece = lax.all_gather(keys, 'ep', axis=0, tiled=True)]
    reduce_scatter x1, waiting for transfers between devices: 0.01 us -> 54.8 us  [local(): lax.psum_scatter(jnp.dot(flat_terms, w_down[0], preferred_element_type=jn...]
    all_gather x0 -> x1, waiting for transfers between devices: none -> 27.8 us  [_post_spot(): upper = jax.lax.all_gather(r1, 'ep', axis=0, tiled=True)]
  transfers between devices with their start and end apart: 3 -> 4, of which waited for: 2 -> 4; matrix products, arithmetic and copies ran while one was open for 4% -> 8% of each run, Pallas kernels for 0% -> 0%
where the time goes in v1:
time: 349 us; the launch traced here: 348 us
  waiting for transfers between devices  182 us (52%)
  blocking collectives  62.6 us (18%)
  local copies, waits for them, and re-layouts  52.1 us (15%)
  matrix products  19.3 us (6%)
  between operations  14 us (4%)
  other arithmetic  11.3 us (3%)
  starting transfers between devices  5.8 us (2%)
    all_gather x1, waiting for transfers between devices, local(): slot_rows = lax.all_gather(arrived[None], 'tp', axis=0, tiled=True)  55.7 us
    all_to_all x1, blocking collectives, local(): lax.all_to_all(outgoing, 'ep', split_axis=0, concat_axis=0, tiled=True)  55.4 us
    reduce_scatter x1, waiting for transfers between devices, local(): lax.psum_scatter(jnp.dot(flat_terms, w_down[0], preferred_element_type=jn...  54.8 us
    all_to_all x1, waiting for transfers between devices, local(): lax.all_to_all(summed, 'ep', split_axis=1, concat_axis=1, tiled=True)[0]  43.2 us
    scatter x1, local copies, waits for them, and re-layouts, fill_slots(): return (blank_slots.at[block_routes, slot_ids].set(copies), slot_ids)  33.4 us
    all_gather x1, waiting for transfers between devices, _post_spot(): upper = jax.lax.all_gather(r1, 'ep', axis=0, tiled=True)  27.8 us
    all_to_all x1, blocking collectives, local(): lax.all_to_all(attn_rows.reshape(positions, q_heads, value_dim), 'tp', sp...  7.21 us
  transfers between devices with their start and end apart: 4, of which 4 were waited for; matrix products, arithmetic and copies ran while one was open for 8% of the time, Pallas kernels for 0%

profile of v1, /device:TPU:0, one launch (start us, length us, event | category | flops | bytes accessed | tf_op | source)
XLA Modules:
  0.0 348.1 jit_solution(3404631823822231410)
XLA Ops:
  7.2 0.8 constant_dynamic-slice_fusion
  9.7 1.2 fusion.24
  10.9 1.3 fusion.26
  12.2 0.6 broadcast_in_dim.60
  12.8 1.2 reshape.233
  14.3 33.4 %scatter_fusion = bf16[8,64,2048]{2,1,0:T(8,128)(2,1)S(1)} fusion(bf16[8,64,2048]{2,1,0:T(8,128)(2,1)S(1)} %broadcast_in_dim.58, s32[256]{0:T(256)S(1)} %reshape.231, bf16[256,2048]{1,0:T(8,128)(2,1)} %reshape.233), kind=kCustom, calls=%fused_computation.1 | custom fusion | bytes 3147776 | tf_op jit(solution)/shard_map/scatter | solution.py:27
  47.7 55.4 %all_to_all.25 = bf16[8,64,2048]{2,1,0:T(8,128)(2,1)} all-to-all(bf16[8,64,2048]{2,1,0:T(8,128)(2,1)S(1)} %scatter_fusion), channel_id=1, replica_groups=mesh['ep'=8,'tp'=4] {'ep'}, dimensions={0} | all-to-all | bytes 4194304 | tf_op jit(solution)/shard_map/all_to_all | solution.py:145
  103.2 0.8 copy-done.2
  104.0 0.7 pad_maximum_fusion
  104.9 55.7 %all-gather.6.cloned.1.call-done = bf16[32,64,2048]{2,1,0:T(8,128)(2,1)} async-done(((bf16[8,64,2048]{2,1,0:T(8,128)(2,1)}), bf16[32,64,2048]{2,1,0:T(8,128)(2,1)}) %all-gather.6.cloned.1.call-update) | async-done | bytes 8388624 | tf_op jit(solution)/shard_map/all_gather | solution.py:146
  160.6 5.9 %fusion.29 = f32[2048,256]{1,0:T(8,128)S(1)} fusion(bf16[2048,2048]{1,0:T(8,128)(2,1)} %bitcast.134, bf16[1,2048,256]{2,1,0:T(8,128)(2,1)S(1)} %copy-done.7), kind=kOutput, calls=%fused_computation.40 | convolution fusion | flops 2147483648 | bytes 11534336 | tf_op jit(solution)/shard_map/dot_general | solution.py:148
  166.6 2.6 fusion.23
  169.2 5.6 %convolution_convert_fusion = bf16[4,8,64,2048]{3,2,1,0:T(8,128)(2,1)} fusion(bf16[4,8,64,256]{3,2,1,0:T(8,128)(2,1)S(1)} %bitcast.130, bf16[1,256,2048]{2,1,0:T(8,128)(2,1)S(1)} %copy-done), kind=kOutput, calls=%fused_computation.28 | convolution fusion | flops 2151677952 | bytes 10485760 | tf_op jit(solution)/shard_map/dot_general | solution.py:157
  174.8 0.9 copy-done.1
  175.9 27.8 %all-gather.4.cloned.1.call-done = bf16[2048,2,128]{2,0,1:T(8,128)(2,1)} async-done(((bf16[256,2,128]{2,0,1:T(8,128)(2,1)}), bf16[2048,2,128]{2,0,1:T(8,128)(2,1)}) %all-gather.4.cloned.1.call-update) | async-done | bytes 1048592 | tf_op jit(solution)/shard_map/all_gather | solution.py:63
  203.6 1.3 fusion.45
  205.3 0.7 copy.64
  206.3 5.9 %while.15 = (s32[]{:T(128)}, f32[256,1,2,2]{0,2,3,1:T(2,128)S(1)}, f32[256,1,2,2]{0,2,3,1:T(2,128)S(1)}, f32[256,1,2,2,128]{0,4,3,2,1:T(8,128)S(1)}, s32[2]{0:T(...) while((s32[]{:T(128)}, f32[256,1,2,2]{0,2,3,1:T(2,128)S(1)}, ...), condition=%wide.region_5.6_spmd.clone, body=%wide.region_0.5_spmd.clone.sunk | while | flops 411570432 | bytes 15155487 | solution.py:110
  207.6 3.4 conditional.3
  207.6 0.7 iota_add_fusion
  208.5 0.9 fusion.4
  209.4 1.0 fusion.5
  212.7 0.7 broadcast_divide_fusion
  214.3 7.2 %all_to_all.26 = bf16[256,2,128]{2,1,0:T(2,128)(2,1)S(1)} all-to-all(bf16[256,2,128]{2,1,0:T(2,128)(2,1)S(1)} %fusion.37), channel_id=1, replica_groups=mesh['ep'=8,'tp'=4] {'tp'}, dimensions={0} | all-to-all | bytes 262144 | tf_op jit(solution)/shard_map/all_to_all | solution.py:120
  221.5 54.8 %reduce-scatter.2.cloned.1.call-done = bf16[1,8,64,2048]{3,2,1,0:T(8,128)(2,1)} async-done(((bf16[4,8,64,2048]{3,2,1,0:T(8,128)(2,1)}), bf16[1,8,64,2048]{3,2,1,0:T(8,128)(2,1)}) %reduce-scatter.2.cloned.1.call-update) | async-done | bytes 2097168 | tf_op jit(solution)/shard_map/reduce_scatter | solution.py:156
  276.4 5.5 %all-to-all-start.2 = ((bf16[1,8,64,2048]{3,2,0,1:T(8,128)(2,1)}), bf16[1,8,64,2048]{3,2,0,1:T(8,128)(2,1)S(1)}, u32[]{:S(2)}, u32[]{:S(2)}) async-start(bf16[1,8,64,2048]{3,2,0,1:T(8,128)(2,1)} %bitcast.127), calls=%async_computation.3 | async-start | bytes 4194304 | tf_op jit(solution)/shard_map/all_to_all | solution.py:164
  282.0 0.7 constant_dynamic-slice_fusion.1
  283.1 3.7 %convolution_convert_fusion.1 = bf16[64,2048]{1,0:T(8,128)(2,1)} fusion(bf16[64,1024]{1,0:T(8,128)(2,1)S(1)} %reshape.221, bf16[1024,2048]{1,0:T(8,128)(2,1)} %param.22), kind=kOutput, calls=%fused_computation.31 | convolution fusion | flops 268566528 | bytes 4587520 | tf_op jit(solution)/shard_map/dot_general | solution.py:127
  286.8 43.2 %all-to-all-done.2 = bf16[1,8,64,2048]{3,2,0,1:T(8,128)(2,1)S(1)} async-done(((bf16[1,8,64,2048]{3,2,0,1:T(8,128)(2,1)}), bf16[1,8,64,2048]{3,2,0,1:T(8,128)(2,1)S(1)}, u32[]{:S(2)}, u32[]{:S(2)}) %all-to-all-start.2) | async-done | bytes 2097184 | tf_op jit(solution)/shard_map/all_to_all | solution.py:164
  329.9 5.3 %gather_fusion = bf16[256,2048]{1,0:T(8,128)(2,1)} fusion(bf16[8,64,2048]{2,1,0:T(8,128)(2,1)S(1)} %bitcast.126, s32[256]{0:T(256)S(1)} %reshape.225), kind=kCustom, calls=%fused_computation | custom fusion | bytes 2099200 | tf_op jit(solution)/shard_map/gather | solution.py:165
  335.3 2.4 reshape.239
  337.6 3.9 %multiply_reduce_fusion = bf16[128,2048]{1,0:T(8,128)(2,1)} fusion(f32[128,2,2048]{2,1,0:T(2,128)S(1)} %reshape.239, f32[128,2]{1,0:T(8,128)S(1)} %copy.73), kind=kLoop, calls=%fused_computation.32 | loop fusion | flops 786432 | bytes 2622464 | tf_op jit(solution)/shard_map/reduce_sum | solution.py:166
  (66 shorter events, 6.9 us)
Async XLA Ops:
  7.2 162.1 %copy-start = (bf16[1,256,2048]{2,1,0:T(8,128)(2,1)S(1)}, bf16[1,256,2048]{2,1,0:T(8,128)(2,1)}, u32[]{:S(2)}) copy-start(bf16[1,256,2048]{2,1,0:T(8,128)(2,1)} %param.29) | copy-start | bytes 3145732
  7.2 153.4 %all-gather.6.cloned.1.call-start = ((), (), s32[]{:S(2)}) async-start(), calls=%async_computation.6 | async-start | bytes 10485760 | tf_op jit(solution)/shard_map/all_gather | solution.py:146
  103.1 0.8 copy-start.2
  103.1 0.9 copy-start.3
  103.1 57.5 %copy-start.7 = (bf16[1,2048,256]{2,1,0:T(8,128)(2,1)S(1)}, bf16[1,2048,256]{2,1,0:T(8,128)(2,1)}, u32[]{:S(2)}) copy-start(bf16[1,2048,256]{2,1,0:T(8,128)(2,1)} %param.27) | copy-start | bytes 3145732
  103.1 100.5 %all-gather.4.cloned.1.call-start = ((), (), s32[]{:S(2)}) async-start(), calls=%async_computation.4 | async-start | bytes 1179648 | tf_op jit(solution)/shard_map/all_gather | solution.py:63
  104.7 171.7 %reduce-scatter.2.cloned.1.call-start = ((), (), s32[]{:S(2)}) async-start(), calls=%async_computation.5 | async-start | bytes 10485760 | tf_op jit(solution)/shard_map/reduce_scatter | solution.py:156
  160.6 5.9 %copy-start.6 = (bf16[32,64,2048]{2,1,0:T(8,128)(2,1)S(1)}, bf16[32,64,2048]{2,1,0:T(8,128)(2,1)}, u32[]{:S(2)}) copy-start(bf16[32,64,2048]{2,1,0:T(8,128)(2,1)} %all-gather.6.cloned.1.call-done) | copy-start | bytes 25165828
  160.6 6.0 %copy-start.8 = (bf16[1,2048,256]{2,1,0:T(8,128)(2,1)S(1)}, bf16[1,2048,256]{2,1,0:T(8,128)(2,1)}, u32[]{:S(2)}) copy-start(bf16[1,2048,256]{2,1,0:T(8,128)(2,1)} %param.28) | copy-start | bytes 3145732
  174.8 0.9 copy-start.1
  212.3 1.1 copy-start.4
  212.3 1.6 copy-start.5
  276.4 53.6 %all-to-all-start.2 = ((bf16[1,8,64,2048]{3,2,0,1:T(8,128)(2,1)}), bf16[1,8,64,2048]{3,2,0,1:T(8,128)(2,1)S(1)}, u32[]{:S(2)}, u32[]{:S(2)}) async-start(bf16[1,8,64,2048]{3,2,0,1:T(8,128)(2,1)} %bitcast.127), calls=%async_computation.3 | async-start | bytes 4194304 | tf_op jit(solution)/shard_map/all_to_all | solution.py:164
Sparse Core Ops, SparseCore 0:
  103.2 57.2 all-gather.5
  163.3 40.2 all-gather.3
  206.2 70.1 reduce-scatter.1
